TPU v7x, 32 devices: a whole 2x2x4 slice. The times are simulated.
32 devices in a mesh: fs: 16 (over z, y, x), tp: 2 (over core).
Axes of the slice: x: 2, y: 2, z: 4, core: 2. Of those that a mesh axis runs over, the one named last changes fastest.
Arguments:
- tokens: bfloat16 [12288, 2048], P('fs'), may hold values from -6 to 6
- norm_gain: float32 [2048], replicated, may hold values from 0.1 to 1.9
- gate_weight: float32 [2048, 5632], P('fs', 'tp'), may hold values from -0.125 to 0.125
- up_weight: float32 [2048, 5632], P('fs', 'tp'), may hold values from -0.125 to 0.125
- gate_scale: float32 [5632], P('tp'), may hold values from 0.1 to 1.9
- up_scale: float32 [5632], P('tp'), may hold values from 0.1 to 1.9
- down_weight: float32 [5632, 2048], P('tp', 'fs'), may hold values from -0.078125 to 0.078125
- down_scale: float32 [2048], P('tp'), may hold values from 0.1 to 1.9
Outputs:
- mixed: bfloat16 [12288, 2048], P('fs', 'tp')
All inputs are finite; a program needn't handle non-finite values.
Results may differ from a plain program's by a relative error of at most 0.014.
Values may be sent and summed in bfloat16 or wider, within the bound.
A program may use at most 128 MiB of HBM per device.

v0:
```python
import jax
import jax.numpy as jnp
from jax import lax
from jax.experimental import pallas as pl
from jax.experimental.pallas import tpu as pltpu
from jax.sharding import PartitionSpec as P

MESH = pl.DeviceIdType.MESH
NT = (((1,), (1,)), ((), ()))
NN = (((1,), (0,)), ((), ()))


def norm(tokens, norm_gain):
    values = tokens.astype(jnp.float32)
    return (
        values * lax.rsqrt(jnp.mean(values * values, axis=-1, keepdims=True) + 1e-06) * norm_gain
    ).astype(jnp.bfloat16)


def gathered(tokens, norm_gain, gate_weight, up_weight, gate_scale, up_scale, down_weight, down_scale):
    normed = norm(tokens, norm_gain)

    def add_rows(piece):
        return jnp.dot(normed, piece, preferred_element_type=jnp.float32)

    gate = add_rows(lax.all_gather(gate_weight.astype(jnp.bfloat16), "fs", axis=0, tiled=True))
    up = add_rows(lax.all_gather(up_weight.astype(jnp.bfloat16), "fs", axis=0, tiled=True))
    hidden = (jax.nn.silu(gate * gate_scale) * (up * up_scale)).astype(jnp.bfloat16)
    terms = jnp.dot(
        hidden,
        lax.all_gather(down_weight.astype(jnp.bfloat16), "fs", axis=1, tiled=True),
        preferred_element_type=jnp.float32,
    )
    summed = lax.psum_scatter(
        terms.astype(jnp.bfloat16), "tp", scatter_dimension=1, tiled=True
    ).astype(jnp.float32)
    return (summed * down_scale).astype(jnp.bfloat16)


def kernel(
    gu_ref, d_ref, xn_ref, gs_ref, us_ref, ds_ref, out_ref,
    xbuf, wgu, wd, accg, accu, hid, pbuf, rbuf,
    lw_sem, lx_sem, rsh_send, rsh_recv, x_send, x_recv, xf_send, xf_recv,
    z_send, z_recv, p_send, p_recv, r_send, r_recv,
):
    f, c = lax.axis_index("fs"), lax.axis_index("tp")
    z, q = lax.div(f, 4), lax.rem(f, 4)
    qk = [q, q + 1 - 2 * lax.rem(q, 2), lax.rem(q + 2, 4), 3 - q]
    part = wd.shape[1]
    width = 4 * wd.shape[2]
    rows = xn_ref.shape[0]
    half = rows // 2
    tile = rows // 3
    tiles = rows // tile
    partner = (f, 1 - c)

    def at(k):
        return (4 * z + qk[k], c)

    def rcopy(src, dst, ssem, rsem, dev):
        return pltpu.make_async_remote_copy(
            src_ref=src, dst_ref=dst, send_sem=ssem, recv_sem=rsem,
            device_id=dev, device_id_type=MESH,
        )

    barrier = pltpu.get_barrier_semaphore()

    def greet(dev):
        pl.semaphore_signal(barrier, inc=1, device_id=dev, device_id_type=MESH)

    greet(partner)
    for k in (1, 2, 3):
        greet(at(k))
    pl.when(z > 0)(lambda: greet((f - 4, c)))
    pl.when(z < 3)(lambda: greet((f + 4, c)))

    slot = [wgu, wd]

    def stored(cls, k):
        cut = pl.ds(pl.multiple_of(qk[k] * part, 16), part)
        return gu_ref.at[:, cut, :] if cls == 0 else d_ref.at[cut, :]

    def own(cls):
        return pltpu.make_async_copy(stored(cls, 0), slot[cls].at[f], lw_sem.at[cls])

    def rsh(cls, k, landing):
        return rcopy(
            stored(cls, k), slot[cls].at[landing],
            rsh_send.at[cls, k - 1], rsh_recv.at[cls, k - 1], at(k),
        )

    mine = pl.ds(pl.multiple_of(half * c, 16), half)
    theirs = pl.ds(pl.multiple_of(half * (1 - c), 16), half)

    def xcopy(k, landing):
        return rcopy(
            xn_ref.at[mine, :], xbuf.at[landing, mine, :],
            x_send.at[k - 1], x_recv.at[k - 1], at(k),
        )

    def xshare(k, cut):
        return rcopy(
            xbuf.at[qk[k], mine, :], xbuf.at[qk[k], cut, :],
            xf_send.at[k - 1], xf_recv.at[k - 1], partner,
        )

    local_x = pltpu.make_async_copy(xn_ref, xbuf.at[q], lx_sem)

    def zcopy(cls, i, d):
        dev = (f + 4, c) if d == 0 else (f - 4, c)
        return rcopy(slot[cls].at[i], slot[cls].at[i], z_send.at[d, cls, i], z_recv.at[cls, i], dev)

    def up_down(cls, i):
        pl.when(z < 3)(lambda: zcopy(cls, i, 0).start())
        pl.when(z > 0)(lambda: zcopy(cls, i, 1).start())

    def relay(cls, r):
        for k in range(4):
            low = 4 * (z - r) + qk[k]
            high = 4 * (z + r) + qk[k]

            @pl.when(z >= r)
            def _():
                zcopy(cls, low, 0).wait_recv()
                if r < 3:
                    pl.when(z < 3)(lambda: zcopy(cls, low, 0).start())

            @pl.when(z + r <= 3)
            def _():
                zcopy(cls, high, 1).wait_recv()
                if r < 3:
                    pl.when(z > 0)(lambda: zcopy(cls, high, 1).start())

    own(0).start()
    own(1).start()
    local_x.start()
    pl.semaphore_wait(barrier, 4 + jnp.minimum(z, 1) + jnp.minimum(3 - z, 1))

    for cls in (0, 1):
        for k in (1, 2, 3):
            rsh(cls, k, f).start()
    for k in (1, 2, 3):
        xcopy(k, q).start()
    own(0).wait()
    up_down(0, f)
    for k in (1, 2, 3):
        rsh(0, k, 4 * z + qk[k]).wait_recv()
        up_down(0, 4 * z + qk[k])
    relay(0, 1)
    relay(0, 2)
    own(1).wait()
    up_down(1, f)
    for k in (1, 2, 3):
        rsh(1, k, 4 * z + qk[k]).wait_recv()
        up_down(1, 4 * z + qk[k])
    for k in (1, 2, 3):
        xcopy(k, qk[k]).wait_recv()
        xshare(k, mine).start()
    local_x.wait()
    relay(1, 1)
    for k in (1, 2, 3):
        xshare(k, theirs).wait_recv()

    side = lax.div(z, 2)
    zz = z + side * (3 - 2 * z)

    def turn(t):
        base = t if t >= 2 else lax.rem(t + zz, 2)
        return base + side * (3 - 2 * base)

    def columns(s):
        return pl.ds(pl.multiple_of(s * width, 128), width)

    def gate_up(t):
        s = turn(t)

        def step(m, _):
            there = pl.ds(pl.multiple_of(lax.rem(m, tiles) * tile, 16), tile)
            here = pl.ds(pl.multiple_of(m * tile, 16), tile)
            x = xbuf[lax.div(m, tiles), there, columns(s)]
            found = []
            for j, acc in enumerate((accg, accu)):
                w = jnp.concatenate([wgu[4 * s + k, j] for k in range(4)], axis=1)
                part_sum = lax.dot_general(x, w, NT, preferred_element_type=jnp.float32)
                if t > 0:
                    part_sum = part_sum + acc[here, :]
                if t < 3:
                    acc[here, :] = part_sum
                found.append(part_sum)
            if t == 3:
                g = found[0] * gs_ref[...]
                u = found[1] * us_ref[...]
                hid[here, :] = (g / (1.0 + jnp.exp(-g)) * u).astype(jnp.bfloat16)
            return 0

        lax.fori_loop(0, 4 * tiles, step, 0)

    gate_up(0)
    gate_up(1)
    relay(1, 2)
    gate_up(2)
    relay(0, 3)
    gate_up(3)
    for k in (1, 2, 3):
        xshare(k, mine).wait_send()

    order = (3, 1, 2, 0)

    def pcopy(s, k):
        i = lax.rem(s, 2)
        return rcopy(
            xbuf.at[qk[k], :, columns(s)], pbuf.at[i, qk[k]],
            p_send.at[i, qk[k]], p_recv.at[i, qk[k]], partner,
        )

    def scopy(s, k):
        i = lax.rem(s, 2)
        return rcopy(
            xbuf.at[qk[k], :, columns(s)], rbuf.at[i, k - 1],
            r_send.at[i, k - 1], r_recv.at[i, k - 1], at(k),
        )

    def finish(s, k):
        @pl.when(lax.div(s, 2) == c)
        def _():
            pcopy(s, k).wait_recv()

            def step(m, _):
                here = pl.ds(pl.multiple_of(m * tile, 16), tile)
                both = xbuf[qk[k], here, columns(s)].astype(jnp.float32) + pbuf[
                    lax.rem(s, 2), qk[k], here, :
                ].astype(jnp.float32)
                xbuf[qk[k], here, columns(s)] = both.astype(jnp.bfloat16)
                return 0

            lax.fori_loop(0, tiles, step, 0)
            if k:
                scopy(s, k).start()

    def down(t):
        s = turn(t)
        for n, k in enumerate(order):
            def step(m, _):
                here = pl.ds(pl.multiple_of(m * tile, 16), tile)
                h = hid[pl.ds(pl.multiple_of(qk[k] * rows + m * tile, 16), tile), :]
                w = jnp.concatenate([wd[4 * s + j] for j in range(4)], axis=1)
                o = lax.dot_general(h, w, NN, preferred_element_type=jnp.float32)
                xbuf[qk[k], here, columns(s)] = o.astype(jnp.bfloat16)
                return 0

            lax.fori_loop(0, tiles, step, 0)
            pl.when(lax.div(s, 2) != c)(lambda: pcopy(s, k).start())
            if n:
                finish(s, order[n - 1])
        finish(s, order[-1])

    down(0)
    down(1)
    down(2)
    relay(1, 3)
    down(3)

    for i in range(2):
        s = 2 * c + i
        for k in (1, 2, 3):
            scopy(s, k).wait_recv()

        def step(m, _):
            here = pl.ds(pl.multiple_of(m * tile, 16), tile)
            total = xbuf[q, here, columns(s)].astype(jnp.float32)
            for k in range(3):
                total = total + rbuf[i, k, here, :].astype(jnp.float32)
            cols = slice(i * width, (i + 1) * width)
            out_ref[here, cols] = (total * ds_ref[:, cols]).astype(jnp.bfloat16)
            return 0

        lax.fori_loop(0, tiles, step, 0)

    for cls in (0, 1):
        for k in (1, 2, 3):
            rsh(cls, k, f).wait_send()
        for r in range(3):
            for k in range(4):
                low, high = 4 * (z - r) + qk[k], 4 * (z + r) + qk[k]
                pl.when((z >= r) & (z < 3))(lambda: zcopy(cls, low, 0).wait_send())
                pl.when((z + r <= 3) & (z > 0))(lambda: zcopy(cls, high, 1).wait_send())
    for k in (1, 2, 3):
        xcopy(k, q).wait_send()
    for i in range(2):
        for k in range(4):
            pcopy(2 * (1 - c) + i, k).wait_send()
            if k:
                scopy(2 * c + i, k).wait_send()


def planes(tokens, norm_gain, gate_weight, up_weight, gate_scale, up_scale, down_weight, down_scale):
    rows, model = tokens.shape
    block, units = gate_weight.shape
    part, width = units // 4, 4 * block
    normed = norm(tokens, norm_gain)
    gu = jnp.stack([gate_weight.astype(jnp.bfloat16).T, up_weight.astype(jnp.bfloat16).T])
    low = down_weight.astype(jnp.bfloat16)
    first = lax.rem(lax.axis_index("fs"), 4) * part
    gs = lax.dynamic_slice(gate_scale, (first,), (part,))[None]
    us = lax.dynamic_slice(up_scale, (first,), (part,))[None]
    bf, f32, dma = jnp.bfloat16, jnp.float32, pltpu.SemaphoreType.DMA
    hbm = pl.BlockSpec(memory_space=pl.ANY)
    vmem = pl.BlockSpec(memory_space=pltpu.VMEM)
    return pl.pallas_call(
        kernel,
        out_shape=jax.ShapeDtypeStruct((rows, down_scale.shape[0]), bf),
        in_specs=[hbm, hbm, hbm, vmem, vmem, vmem],
        out_specs=vmem,
        scratch_shapes=[
            pltpu.VMEM((4, rows, model), bf),
            pltpu.VMEM((16, 2, part, block), bf),
            pltpu.VMEM((16, part, block), bf),
            pltpu.VMEM((4 * rows, part), f32),
            pltpu.VMEM((4 * rows, part), f32),
            pltpu.VMEM((4 * rows, part), bf),
            pltpu.VMEM((2, 4, rows, width), bf),
            pltpu.VMEM((2, 3, rows, width), bf),
            dma((2,)), dma, dma((2, 3)), dma((2, 3)),
            dma((3,)), dma((3,)), dma((3,)), dma((3,)),
            dma((2, 2, 16)), dma((2, 16)),
            dma((2, 4)), dma((2, 4)), dma((2, 3)), dma((2, 3)),
        ],
        compiler_params=pltpu.CompilerParams(
            collective_id=0, has_side_effects=True, vmem_limit_bytes=67043328
        ),
    )(gu, low, normed, gs, us, down_scale[None])


def solution(mesh):
    in_specs = (
        P("fs", None),
        P(),
        P("fs", "tp"),
        P("fs", "tp"),
        P("tp"),
        P("tp"),
        P("tp", "fs"),
        P("tp"),
    )
    out_specs = P("fs", "tp")
    body = planes if (mesh.shape["fs"], mesh.shape["tp"]) == (16, 2) else gathered
    return jax.shard_map(body, mesh=mesh, in_specs=in_specs, out_specs=out_specs, check_vma=False)
```

profile of v0, /device:TPU:1, one launch (start us, length us, event | category | flops | bytes accessed | tf_op | source)
XLA Modules:
  0.0 241.7 jit_solution(18257722815815014564)
XLA Ops:
  0.0 0.0 copy-start.1
  0.0 0.9 dynamic_slice.6
  0.9 0.6 broadcast_in_dim.11.gs_ref
  1.5 0.8 dynamic_slice.7
  2.3 0.6 broadcast_in_dim.12.us_ref
  2.8 2.6 %fusion = f32[768]{0:T(1024)S(1)} fusion(bf16[768,2048]{1,0:T(8,128)(2,1)} %param.8), kind=kLoop, calls=%fused_computation.2 | loop fusion | flops 4717824 | bytes 3148800 | tf_op jit(solution)/shard_map/reduce_sum | solution.py:16
  5.4 0.0 copy-done.1
  5.4 1.1 copy.9
  6.6 0.0 copy-start
  6.6 0.0 copy-start.3
  6.6 2.6 %copy.10 = bf16[128,2816]{0,1:T(8,128)(2,1)} copy(f32[128,2816]{1,0:T(8,128)} %param.11) | data formatting | bytes 2162688 | tf_op args[3]
  9.2 0.0 copy-start.2
  9.2 2.7 %pad_maximum_fusion.gu_ref = bf16[2,2816,128]{2,1,0:T(8,128)(2,1)} fusion(bf16[1,2816,128]{2,1,0:T(8,128)(2,1)} %bitcast.12, bf16[1,2816,128]{2,1,0:T(8,128)(2,1)} %bitcast.11), kind=kLoop, calls=%fused_computation.5 | loop fusion | flops 720896 | bytes 2883584 | tf_op jit(solution)/shard_map/stack | solution.py:301
  11.9 0.0 copy-done.2
  11.9 0.9 convert_element_type.17.d_ref
  12.8 0.0 copy-done
  12.8 0.0 copy-done.3
  12.8 2.4 %fusion.2.xn_ref = bf16[768,2048]{1,0:T(8,128)(2,1)} fusion(bf16[768,2048]{1,0:T(8,128)(2,1)S(1)} %copy-done, f32[2048]{0:T(1024)S(1)} %copy-done.3, f32[768]{0:T(1024)S(1)} %add_rsqrt_fusion), kind=kLoop, calls=%fused_computation.4 | loop fusion | flops 6291456 | bytes 6302720 | tf_op jit(solution)/shard_map/convert_element_type | solution.py:17
  15.3 223.8 %shard_map.82 = bf16[768,1024]{1,0:T(8,128)(2,1)} custom-call(bf16[2,2816,128]{2,1,0:T(8,128)(2,1)} %pad_maximum_fusion.gu_ref, bf16[2816,128]{1,0:T(8,128)(2,1)} %convert_element_type.17.d_ref, bf16[768,2048]{1,0:T(8,128)(2,1)} %fusion.2.xn_ref, f32[1,704]{1,0:T(1,128)} %broadcast_in_dim.11.gs_ref, f32[1,704]{1,0:T(1,128)} %broadcast_in_dim.12.us_ref, ...), custom_call_target="tpu_custom_call" | custom-call | tf_op jit(solution)/shard_map/pallas_call | solution.py:309
  239.1 2.7 %copy.12 = bf16[768,1024]{1,0:T(8,128)(2,1)} copy(bf16[768,1024]{1,0:T(8,128)(2,1)} %shard_map.82) | data formatting | bytes 3145728
  (1 shorter events, 0.0 us)
Async XLA Ops:
  0.0 5.4 %copy-start.1 = (f32[128,2816]{1,0:T(8,128)S(1)}, f32[128,2816]{1,0:T(8,128)}, u32[]{:S(2)}) copy-start(f32[128,2816]{1,0:T(8,128)} %param.10) | copy-start | bytes 4325380
  6.6 6.3 %copy-start = (bf16[768,2048]{1,0:T(8,128)(2,1)S(1)}, bf16[768,2048]{1,0:T(8,128)(2,1)}, u32[]{:S(2)}) copy-start(bf16[768,2048]{1,0:T(8,128)(2,1)} %param.8) | copy-start | bytes 9437188
  6.6 6.3 %copy-start.3 = (f32[2048]{0:T(1024)S(1)}, f32[2048]{0:T(1024)}, u32[]{:S(2)}) copy-start(f32[2048]{0:T(1024)} %param.9) | copy-start | bytes 24580
  9.2 2.7 %copy-start.2 = (f32[2816,128]{1,0:T(8,128)S(1)}, f32[2816,128]{1,0:T(8,128)}, u32[]{:S(2)}) copy-start(f32[2816,128]{1,0:T(8,128)} %param.14) | copy-start | bytes 4325380
where the time goes:
time: 242 us
  Pallas kernels  224 us (93%)
  local copies, waits for them, and re-layouts  9.29 us (4%)
  other arithmetic  8.63 us (4%)
    pallas_call x1, Pallas kernels, planes(): pl.pallas_call(kernel, out_shape=jax.ShapeDtypeStruct((rows, down_scale.s...  224 us
    unnamed x11, local copies, waits for them, and re-layouts  6.47 us

commit v1 on v0

v1 whole, which is shorter than its diff:
```python
import jax
import jax.numpy as jnp
from jax import lax
from jax.experimental import pallas as pl
from jax.experimental.pallas import tpu as pltpu
from jax.sharding import PartitionSpec as P

MESH = pl.DeviceIdType.MESH
NN = (((1,), (0,)), ((), ()))
TILE = 128


def norm(tokens, norm_gain):
    values = tokens.astype(jnp.float32)
    return (
        values * lax.rsqrt(jnp.mean(values * values, axis=-1, keepdims=True) + 1e-06) * norm_gain
    ).astype(jnp.bfloat16)


def gathered(tokens, norm_gain, gate_weight, up_weight, gate_scale, up_scale, down_weight, down_scale):
    normed = norm(tokens, norm_gain)

    def add_rows(piece):
        return jnp.dot(normed, piece, preferred_element_type=jnp.float32)

    gate = add_rows(lax.all_gather(gate_weight.astype(jnp.bfloat16), "fs", axis=0, tiled=True))
    up = add_rows(lax.all_gather(up_weight.astype(jnp.bfloat16), "fs", axis=0, tiled=True))
    hidden = (jax.nn.silu(gate * gate_scale) * (up * up_scale)).astype(jnp.bfloat16)
    terms = jnp.dot(
        hidden,
        lax.all_gather(down_weight.astype(jnp.bfloat16), "fs", axis=1, tiled=True),
        preferred_element_type=jnp.float32,
    )
    summed = lax.psum_scatter(
        terms.astype(jnp.bfloat16), "tp", scatter_dimension=1, tiled=True
    ).astype(jnp.float32)
    return (summed * down_scale).astype(jnp.bfloat16)


def kernel(
    g_ref, u_ref, d_ref, x_ref, ng_ref, gs_ref, us_ref, ds_ref, out_ref,
    xbuf, wgu, wd, gsend, dsend, accg, accu, hid, pbuf, rbuf, scl,
    l_sem, rsh_send, rsh_recv, x_send, x_recv, s_send, s_recv,
    z_send, z_recv, p_send, p_recv, r_send, r_recv,
):
    f, c = lax.axis_index("fs"), lax.axis_index("tp")
    z, q = lax.div(f, 4), lax.rem(f, 4)
    qk = [q, q + 1 - 2 * lax.rem(q, 2), lax.rem(q + 2, 4), 3 - q]
    tiles = gsend.shape[1]
    hi = wgu.shape[2]
    lo = tiles // 4
    rows = x_ref.shape[0]
    half, quarter = rows // 2, rows // 4
    width = 4 * TILE
    pair = 2 * TILE
    big = lax.rem(q + c, 2) == 0
    small = lax.rem(q + c, 2) != 0
    partner = (f, 1 - c)

    def at(k):
        return (4 * z + qk[k], c)

    def first(k):
        return lo * qk[k] + lax.div(qk[k] + 1 - c, 2)

    def chip(k):
        return lax.rem(q + k, 2) + 2 * lax.rem(lax.div(q, 2) + lax.div(k, 2), 2)

    def rcopy(src, dst, ssem, rsem, dev):
        return pltpu.make_async_remote_copy(
            src_ref=src, dst_ref=dst, send_sem=ssem, recv_sem=rsem,
            device_id=dev, device_id_type=MESH,
        )

    barrier = pltpu.get_barrier_semaphore()

    def greet(dev):
        pl.semaphore_signal(barrier, inc=1, device_id=dev, device_id_type=MESH)

    greet(partner)
    for k in (1, 2, 3):
        greet(at(k))
    pl.when(z > 0)(lambda: greet((f - 4, c)))
    pl.when(z < 3)(lambda: greet((f + 4, c)))

    slab = hi * TILE
    cuts = [(i, min(slab, tiles * TILE - i)) for i in range(0, tiles * TILE, slab)]
    loads = ([], [])
    for j, ref in enumerate((g_ref, u_ref)):
        for n, (i, w) in enumerate(cuts):
            loads[j].append(pltpu.make_async_copy(
                ref.at[:, pl.ds(i, w)],
                accg.at[pl.ds((j * len(cuts) + n) * TILE, TILE), pl.ds(0, w)],
                l_sem.at[j, n],
            ))
    load_d = pltpu.make_async_copy(
        d_ref, accu.at[pl.ds(0, tiles * TILE), pl.ds(0, TILE)], l_sem.at[2, 0]
    )
    mine = pl.ds(pl.multiple_of(half * c, 16), half)
    load_x = pltpu.make_async_copy(x_ref.at[mine, :], xbuf.at[q, mine, :], l_sem.at[2, 1])
    for j in (0, 1):
        for copy in loads[j]:
            copy.start()
    load_d.start()
    load_x.start()

    @pl.when(small)
    def _():
        nothing = jnp.zeros((TILE, TILE), jnp.bfloat16)

        def step(i, _):
            wgu[i, 0, hi - 1] = nothing
            wgu[i, 1, hi - 1] = nothing
            wd[i, hi - 1] = nothing
            return 0

        lax.fori_loop(0, 16, step, 0)

    start = first(0)
    for j, ref in enumerate((gs_ref, us_ref)):
        scl[j : j + 1, : lo * TILE] = ref[:, pl.ds(pl.multiple_of(start * TILE, TILE), lo * TILE)]
        last = jnp.minimum(start + lo, tiles - 1)
        scl[j : j + 1, lo * TILE :] = ref[:, pl.ds(pl.multiple_of(last * TILE, TILE), TILE)]

    for j in (0, 1):
        for copy in loads[j]:
            copy.wait()
        for i in range(tiles):
            n, m = divmod(i, hi)
            gsend[j, i] = accg[
                (j * len(cuts) + n) * TILE : (j * len(cuts) + n + 1) * TILE,
                m * TILE : (m + 1) * TILE,
            ].astype(jnp.bfloat16)
        for i in range(lo):
            wgu[f, j, i] = gsend[j, start + i]

    @pl.when(big)
    def _():
        for j in (0, 1):
            wgu[f, j, hi - 1] = gsend[j, start + hi - 1]

    slot = [wgu, wd]

    def cut(cls, i, n):
        return wgu.at[i, :, pl.ds(0, n)] if cls == 0 else wd.at[i, pl.ds(0, n)]

    def stored(cls, k, n):
        return gsend.at[:, pl.ds(first(k), n)] if cls == 0 else dsend.at[pl.ds(first(k), n)]

    def sized(fn):
        pl.when(big)(lambda: fn(hi))
        pl.when(small)(lambda: fn(lo))

    def swapped(fn):
        pl.when(small)(lambda: fn(hi))
        pl.when(big)(lambda: fn(lo))

    def rsh(cls, k, n):
        return rcopy(
            stored(cls, k, n), cut(cls, f, n),
            rsh_send.at[cls, k - 1], rsh_recv.at[cls, k - 1], at(k),
        )

    def rsh_arrived(cls, k, n):
        where = cut(cls, 4 * z + qk[k], n)
        return rcopy(where, where, rsh_send.at[cls, k - 1], rsh_recv.at[cls, k - 1], at(k))

    def rsh_start(cls, k):
        (sized if k == 2 else swapped)(lambda n: rsh(cls, k, n).start())

    def rsh_wait_send(cls, k):
        (sized if k == 2 else swapped)(lambda n: rsh(cls, k, n).wait_send())

    def rsh_wait(cls, k):
        sized(lambda n: rsh_arrived(cls, k, n).wait_recv())

    def zcopy(cls, i, d, n):
        dev = (f + 4, c) if d == 0 else (f - 4, c)
        return rcopy(cut(cls, i, n), cut(cls, i, n), z_send.at[d, cls, i], z_recv.at[cls, i], dev)

    def inward(cls, i):
        pl.when(z < 2)(lambda: sized(lambda n: zcopy(cls, i, 0, n).start()))
        pl.when(z > 1)(lambda: sized(lambda n: zcopy(cls, i, 1, n).start()))

    def outward(cls, i):
        pl.when(z == 2)(lambda: sized(lambda n: zcopy(cls, i, 0, n).start()))
        pl.when(z == 1)(lambda: sized(lambda n: zcopy(cls, i, 1, n).start()))

    def relay(cls, r, ks):
        for k in ks:
            low = 4 * (z - r) + qk[k]
            high = 4 * (z + r) + qk[k]

            @pl.when(z >= r)
            def _():
                sized(lambda n: zcopy(cls, low, 0, n).wait_recv())
                if r < 3:
                    pl.when(z < 3)(lambda: sized(lambda n: zcopy(cls, low, 0, n).start()))

            @pl.when(z + r <= 3)
            def _():
                sized(lambda n: zcopy(cls, high, 1, n).wait_recv())
                if r < 3:
                    pl.when(z > 0)(lambda: sized(lambda n: zcopy(cls, high, 1, n).start()))

    pl.semaphore_wait(barrier, 4 + jnp.minimum(z, 1) + jnp.minimum(3 - z, 1))
    outward(0, f)
    inward(0, f)
    for k in (1, 2, 3):
        rsh_start(0, k)

    load_d.wait()
    for i in range(tiles):
        dsend[i] = accu[i * TILE : (i + 1) * TILE, :TILE].astype(jnp.bfloat16)
    for i in range(lo):
        wd[f, i] = dsend[start + i]

    @pl.when(big)
    def _():
        wd[f, hi - 1] = dsend[start + hi - 1]

    load_x.wait()

    def normalize(m, _):
        here = pl.ds(pl.multiple_of(half * c + m * 16, 16), 16)
        values = xbuf[q, here, :].astype(jnp.float32)
        scale = lax.rsqrt(jnp.mean(values * values, axis=-1, keepdims=True) + 1e-06)
        xbuf[q, here, :] = (values * scale * ng_ref[...]).astype(jnp.bfloat16)
        return 0

    lax.fori_loop(0, half // 16, normalize, 0)

    def piece(core, h):
        return pl.ds(pl.multiple_of(half * core + h * quarter, 16), quarter)

    def xcopy(owner, h, ssem, rsem, dev):
        where = xbuf.at[qk[owner], piece(c, h), :]
        return rcopy(where, where, ssem, rsem, dev)

    def direct(k, h, owner):
        return xcopy(owner, h, x_send.at[k - 1, h], x_recv.at[k - 1, h], at(k))

    def onward(h, owner):
        return xcopy(owner, h, x_send.at[2, h], x_recv.at[2, h], at(2 if h == 0 else 1))

    def share(k, h, core):
        where = xbuf.at[qk[k], piece(core, h), :]
        return rcopy(where, where, s_send.at[k, h], s_recv.at[k, h], partner)

    outward(1, f)
    inward(1, f)
    for k in (1, 2, 3):
        rsh_start(1, k)
    direct(1, 0, 0).start()
    direct(2, 1, 0).start()
    direct(1, 1, 0).start()
    direct(2, 0, 0).start()
    for h in (0, 1):
        share(0, h, c).start()

    for k in (1, 2, 3):
        rsh_wait(0, k)
        outward(0, 4 * z + qk[k])
        inward(0, 4 * z + qk[k])

    side = lax.div(z, 2)
    zz = z + side * (3 - 2 * z)

    def turn(t):
        base = t if t >= 2 else lax.rem(t + zz, 2)
        return base + side * (3 - 2 * base)

    def columns(s, h=None):
        if h is None:
            return pl.ds(pl.multiple_of(s * width, TILE), width)
        return pl.ds(pl.multiple_of(s * width + h * pair, TILE), pair)

    def gate_up(t, k0, k1):
        s = turn(t)

        def step(m, _):
            who = chip(lax.div(m, hi // 2))
            n = lax.rem(m, hi // 2)
            here = pl.ds(pl.multiple_of(who * rows, 16), rows)
            cols = pl.ds(pl.multiple_of(n * pair, TILE), pair)
            found = []
            for j, acc in enumerate((accg, accu)):
                w = jnp.concatenate([
                    jnp.concatenate([wgu[4 * s + i, j, 2 * n], wgu[4 * s + i, j, 2 * n + 1]], axis=1)
                    for i in range(4)
                ], axis=0)
                x = xbuf[who, :, columns(s)]
                part_sum = lax.dot_general(x, w, NN, preferred_element_type=jnp.float32)
                if t > 0:
                    part_sum = part_sum + acc[here, cols]
                if t < 3:
                    acc[here, cols] = part_sum
                found.append(part_sum)
            if t == 3:
                g = found[0] * scl[0:1, cols]
                u = found[1] * scl[1:2, cols]
                hid[here, cols] = (g / (1.0 + jnp.exp(-g)) * u).astype(jnp.bfloat16)
            return 0

        lax.fori_loop(k0 * (hi // 2), k1 * (hi // 2), step, 0)

    relay(0, 1, range(4))
    for h in (0, 1):
        share(0, h, 1 - c).wait_recv()
    direct(1, 0, 1).wait_recv()
    onward(0, 1).start()
    share(1, 0, c).start()
    direct(2, 1, 2).wait_recv()
    onward(1, 2).start()
    share(2, 1, c).start()
    for k in (1, 2, 3):
        rsh_wait(1, k)
        inward(1, 4 * z + qk[k])
    relay(0, 2, range(3))
    direct(1, 1, 1).wait_recv()
    share(1, 1, c).start()
    direct(2, 0, 2).wait_recv()
    share(2, 0, c).start()
    for k in (1, 2):
        for h in (0, 1):
            share(k, h, 1 - c).wait_recv()
    gate_up(0, 0, 3)
    relay(0, 2, range(3, 4))
    for k in (1, 2, 3):
        outward(1, 4 * z + qk[k])
    gate_up(1, 0, 3)
    gate_up(2, 0, 3)
    onward(0, 3).wait_recv()
    share(3, 0, c).start()
    onward(1, 3).wait_recv()
    share(3, 1, c).start()
    for h in (0, 1):
        share(3, h, 1 - c).wait_recv()
    gate_up(0, 3, 4)
    gate_up(1, 3, 4)
    gate_up(2, 3, 4)
    for h in (0, 1):
        direct(1, h, 0).wait_send()
        direct(2, h, 0).wait_send()
        onward(h, 1 + h).wait_send()
        for k in range(4):
            share(k, h, c).wait_send()
    relay(0, 3, range(4))
    gate_up(3, 0, 4)

    order = (3, 1, 2, 0)

    def pcopy(s, k):
        i = lax.rem(s, 2)
        return rcopy(
            xbuf.at[qk[k], :, columns(s)], pbuf.at[i, k],
            p_send.at[i, k], p_recv.at[i, k], partner,
        )

    places = ((1, 0, 1), (3, 0, 1), (2, 1, 2), (3, 1, 2), (2, 0, 2), (1, 1, 1))

    def scopy(s, place):
        i = lax.rem(s, 2)
        k, h, to = places[place]
        return rcopy(
            xbuf.at[qk[k], :, columns(s, h)], rbuf.at[i, place],
            r_send.at[i, place], r_recv.at[i, place], at(to),
        )

    def added(where, cols, more):
        def step(m, _):
            here = pl.ds(pl.multiple_of(m * TILE, 16), TILE)
            both = xbuf[where, here, cols].astype(jnp.float32) + more[here, :].astype(jnp.float32)
            xbuf[where, here, cols] = both.astype(jnp.bfloat16)
            return 0

        lax.fori_loop(0, rows // TILE, step, 0)

    def finish(s, k):
        @pl.when(lax.div(s, 2) == c)
        def _():
            pcopy(s, k).wait_recv()
            added(qk[k], columns(s), pbuf.at[lax.rem(s, 2), k])
            for place in range(4):
                if places[place][0] == k:
                    scopy(s, place).start()

    def down(t):
        s = turn(t)
        for n, k in enumerate(order):
            here = pl.ds(pl.multiple_of(qk[k] * rows, 16), rows)

            def step(h, _):
                w = jnp.concatenate(
                    [wd[4 * s + 2 * h + i].reshape(hi * TILE, TILE) for i in (0, 1)], axis=1
                )
                o = lax.dot_general(hid[here, :], w, NN, preferred_element_type=jnp.float32)
                xbuf[qk[k], :, columns(s, h)] = o.astype(jnp.bfloat16)
                return 0

            lax.fori_loop(0, 2, step, 0)
            pl.when(lax.div(s, 2) != c)(lambda: pcopy(s, k).start())
            if n:
                finish(s, order[n - 1])
        finish(s, order[-1])

    def second(t):
        s = turn(t)

        @pl.when(lax.div(s, 2) == c)
        def _():
            i = lax.rem(s, 2)
            for came, goes in ((1, 4), (3, 5)):
                scopy(s, came).wait_recv()
                k, h, _ = places[goes]
                added(qk[k], columns(s, h), rbuf.at[i, came])
                scopy(s, goes).start()

    def result(i, h):
        s = 2 * c + i
        cols = pl.ds(pl.multiple_of(i * width + h * pair, TILE), pair)
        return pltpu.make_async_copy(xbuf.at[q, :, columns(s, h)], out_ref.at[:, cols], l_sem.at[i, h])

    def final(t):
        s = turn(t)

        @pl.when(lax.div(s, 2) == c)
        def _():
            i = lax.rem(s, 2)
            for h, (one, two) in enumerate(((0, 4), (2, 5))):
                scopy(s, one).wait_recv()
                scopy(s, two).wait_recv()
                cols = pl.ds(pl.multiple_of(i * width + h * pair, TILE), pair)

                def step(m, _):
                    here = pl.ds(pl.multiple_of(m * TILE, 16), TILE)
                    total = (
                        xbuf[q, here, columns(s, h)].astype(jnp.float32)
                        + rbuf[i, one, here, :].astype(jnp.float32)
                        + rbuf[i, two, here, :].astype(jnp.float32)
                    )
                    xbuf[q, here, columns(s, h)] = (total * ds_ref[:, cols]).astype(jnp.bfloat16)
                    return 0

                lax.fori_loop(0, rows // TILE, step, 0)
                result(i, h).start()

    down(0)
    relay(1, 1, range(4))
    down(1)
    second(0)
    relay(1, 2, range(4))
    down(2)
    second(1)
    second(2)
    relay(1, 3, range(4))
    down(3)
    final(0)
    final(1)
    final(2)
    second(3)
    final(3)

    for cls in (0, 1):
        for k in (1, 2, 3):
            rsh_wait_send(cls, k)
        for r in range(3):
            for k in range(4):
                low, high = 4 * (z - r) + qk[k], 4 * (z + r) + qk[k]
                pl.when((z >= r) & (z < 3))(
                    lambda: sized(lambda n: zcopy(cls, low, 0, n).wait_send())
                )
                pl.when((z + r <= 3) & (z > 0))(
                    lambda: sized(lambda n: zcopy(cls, high, 1, n).wait_send())
                )
    for i in range(2):
        for h in (0, 1):
            result(i, h).wait()
        for k in range(4):
            pcopy(2 * (1 - c) + i, k).wait_send()
        for place in range(6):
            scopy(2 * c + i, place).wait_send()


def planes(tokens, norm_gain, gate_weight, up_weight, gate_scale, up_scale, down_weight, down_scale):
    rows, model = tokens.shape
    units = gate_weight.shape[1]
    tiles = units // TILE
    hi = -(-tiles // 4)
    bf, f32, dma = jnp.bfloat16, jnp.float32, pltpu.SemaphoreType.DMA
    hbm = pl.BlockSpec(memory_space=pl.ANY)
    vmem = pl.BlockSpec(memory_space=pltpu.VMEM)
    return pl.pallas_call(
        kernel,
        out_shape=jax.ShapeDtypeStruct((rows, down_scale.shape[0]), bf),
        in_specs=[hbm, hbm, hbm, hbm, vmem, vmem, vmem, vmem],
        out_specs=hbm,
        scratch_shapes=[
            pltpu.VMEM((4, rows, model), bf),
            pltpu.VMEM((16, 2, hi, TILE, TILE), bf),
            pltpu.VMEM((16, hi, TILE, TILE), bf),
            pltpu.VMEM((2, tiles, TILE, TILE), bf),
            pltpu.VMEM((tiles, TILE, TILE), bf),
            pltpu.VMEM((4 * rows, hi * TILE), f32),
            pltpu.VMEM((4 * rows, hi * TILE), f32),
            pltpu.VMEM((4 * rows, hi * TILE), bf),
            pltpu.VMEM((2, 4, rows, 4 * TILE), bf),
            pltpu.VMEM((2, 6, rows, 2 * TILE), bf),
            pltpu.VMEM((8, hi * TILE), f32),
            dma((3, 4)), dma((2, 3)), dma((2, 3)),
            dma((3, 2)), dma((3, 2)), dma((4, 2)), dma((4, 2)),
            dma((2, 2, 16)), dma((2, 16)),
            dma((2, 4)), dma((2, 4)), dma((2, 6)), dma((2, 6)),
        ],
        compiler_params=pltpu.CompilerParams(
            collective_id=0, has_side_effects=True, vmem_limit_bytes=67043328
        ),
    )(
        gate_weight, up_weight, down_weight, tokens,
        norm_gain[None], gate_scale[None], up_scale[None], down_scale[None],
    )


def solution(mesh):
    in_specs = (
        P("fs", None),
        P(),
        P("fs", "tp"),
        P("fs", "tp"),
        P("tp"),
        P("tp"),
        P("tp", "fs"),
        P("tp"),
    )
    out_specs = P("fs", "tp")
    body = planes if (mesh.shape["fs"], mesh.shape["tp"]) == (16, 2) else gathered
    return jax.shard_map(body, mesh=mesh, in_specs=in_specs, out_specs=out_specs, check_vma=False)
```

time: 242 us -> 181 us (0.75)
  Pallas kernels: 224 us -> 175 us
  other arithmetic: 8.63 us -> 0 us
  local copies, waits for them, and re-layouts: 9.29 us -> 5.29 us
    pallas_call x1, Pallas kernels: 224 us -> 175 us  [planes(): pl.pallas_call(kernel, out_shape=jax.ShapeDtypeStruct((rows, down_scale.s...]
    unnamed x11 -> x1, local copies, waits for them, and re-layouts: 6.47 us -> 2.67 us
    convert_element_type x2 -> x0, other arithmetic: 3.38 us -> none  [the longest x1 2.44 us: norm(): return (values * lax.rsqrt(jnp.mean(values * values, axis=-1, keepdims=Tr...]
    another operation x1 -> x0, other arithmetic: 2.67 us -> none  [planes(): jnp.stack([gate_weight.astype(jnp.bfloat16).T, up_weight.astype(jnp.bfloa...]
    reduce_sum x1 -> x0, other arithmetic: 2.57 us -> none  [norm(): jnp.mean(values * values, axis=-1, keepdims=True) + 1e-06]
where the time goes in v1:
time: 181 us; the launch traced here: 180 us
  Pallas kernels  175 us (97%)
  local copies, waits for them, and re-layouts  5.29 us (3%)
    pallas_call x1, Pallas kernels, planes(): pl.pallas_call(kernel, out_shape=jax.ShapeDtypeStruct((rows, down_scale.s...  175 us

profile of v1, /device:TPU:1, one launch (start us, length us, event | category | flops | bytes accessed | tf_op | source)
XLA Modules:
  0.0 180.4 jit_solution(11312630460282935399)
XLA Ops:
  0.0 1.3 broadcast_in_dim.13.gs_ref
  1.3 1.3 broadcast_in_dim.14.us_ref
  2.6 175.1 %shard_map.82 = bf16[768,1024]{1,0:T(8,128)(2,1)} custom-call(f32[128,2816]{1,0:T(8,128)} %g_ref.1, f32[128,2816]{1,0:T(8,128)} %u_ref.1, f32[2816,128]{1,0:T(8,128)} %d_ref.1, bf16[768,2048]{1,0:T(8,128)(2,1)} %x_ref.1, f32[1,2048]{1,0:T(1,128)} %bitcast.2, f32[1,2816]{1,0:T(1,128)} %broadcast_in_dim.13.gs_ref, f32[1,2816]{1,0:T(1,128)} %broadcast_in_dim.14.us_ref, ...), custom_call_target="tpu_custom_call" | custom-call | tf_op jit(solution)/shard_map/pallas_call | solution.py:493
  177.8 2.7 %copy.10 = bf16[768,1024]{1,0:T(8,128)(2,1)} copy(bf16[768,1024]{1,0:T(8,128)(2,1)} %shard_map.82) | data formatting | bytes 3145728

commit v2 on v1

v2 whole, which is shorter than its diff:
```python
import jax
import jax.numpy as jnp
from jax import lax
from jax.experimental import pallas as pl
from jax.experimental.pallas import tpu as pltpu
from jax.sharding import PartitionSpec as P

MESH = pl.DeviceIdType.MESH
NN = (((1,), (0,)), ((), ()))
TILE = 128


def norm(tokens, norm_gain):
    values = tokens.astype(jnp.float32)
    return (
        values * lax.rsqrt(jnp.mean(values * values, axis=-1, keepdims=True) + 1e-06) * norm_gain
    ).astype(jnp.bfloat16)


def gathered(tokens, norm_gain, gate_weight, up_weight, gate_scale, up_scale, down_weight, down_scale):
    normed = norm(tokens, norm_gain)

    def add_rows(piece):
        return jnp.dot(normed, piece, preferred_element_type=jnp.float32)

    gate = add_rows(lax.all_gather(gate_weight.astype(jnp.bfloat16), "fs", axis=0, tiled=True))
    up = add_rows(lax.all_gather(up_weight.astype(jnp.bfloat16), "fs", axis=0, tiled=True))
    hidden = (jax.nn.silu(gate * gate_scale) * (up * up_scale)).astype(jnp.bfloat16)
    terms = jnp.dot(
        hidden,
        lax.all_gather(down_weight.astype(jnp.bfloat16), "fs", axis=1, tiled=True),
        preferred_element_type=jnp.float32,
    )
    summed = lax.psum_scatter(
        terms.astype(jnp.bfloat16), "tp", scatter_dimension=1, tiled=True
    ).astype(jnp.float32)
    return (summed * down_scale).astype(jnp.bfloat16)


def kernel(
    g_ref, u_ref, d_ref, x_ref, ng_ref, gs_ref, us_ref, ds_ref, out_ref,
    xbuf, wg, wu, wd, gsend, usend, dsend, accg, accu, hid, pbuf, rbuf, scl,
    l_sem, rsh_send, rsh_recv, x_send, x_recv, s_send, s_recv,
    z_send, z_recv, p_send, p_recv, r_send, r_recv,
):
    f, c = lax.axis_index("fs"), lax.axis_index("tp")
    z, q = lax.div(f, 4), lax.rem(f, 4)
    qk = [q, q + 1 - 2 * lax.rem(q, 2), lax.rem(q + 2, 4), 3 - q]
    slot, sends = (wg, wu, wd), (gsend, usend, dsend)
    part = wd.shape[1]
    tiles, full, odd = 4 * part // TILE, part // TILE, part % TILE
    hi = full + 1
    rows = x_ref.shape[0]
    half, quarter = rows // 2, rows // 4
    width = 4 * TILE
    pair = 2 * TILE
    partner = (f, 1 - c)

    def at(k):
        return (4 * z + qk[k], c)

    def chip(k):
        return lax.rem(q + k, 2) + 2 * lax.rem(lax.div(q, 2) + lax.div(k, 2), 2)

    def rcopy(src, dst, ssem, rsem, dev):
        return pltpu.make_async_remote_copy(
            src_ref=src, dst_ref=dst, send_sem=ssem, recv_sem=rsem,
            device_id=dev, device_id_type=MESH,
        )

    barrier = pltpu.get_barrier_semaphore()

    def greet(dev):
        pl.semaphore_signal(barrier, inc=1, device_id=dev, device_id_type=MESH)

    greet(partner)
    for k in (1, 2, 3):
        greet(at(k))
    pl.when(z > 0)(lambda: greet((f - 4, c)))
    pl.when(z < 3)(lambda: greet((f + 4, c)))

    slab = hi * TILE
    cuts = [(i, min(slab, tiles * TILE - i)) for i in range(0, tiles * TILE, slab)]
    loads = ([], [])
    for j, ref in enumerate((g_ref, u_ref)):
        for n, (i, w) in enumerate(cuts):
            loads[j].append(pltpu.make_async_copy(
                ref.at[:, pl.ds(i, w)],
                accg.at[pl.ds((j * len(cuts) + n) * TILE, TILE), pl.ds(0, w)],
                l_sem.at[j, n],
            ))
    load_d = pltpu.make_async_copy(
        d_ref, accu.at[pl.ds(0, tiles * TILE), pl.ds(0, TILE)], l_sem.at[2, 0]
    )
    mine = pl.ds(pl.multiple_of(half * c, 16), half)
    load_x = pltpu.make_async_copy(x_ref.at[mine, :], xbuf.at[q, mine, :], l_sem.at[2, 1])
    for copy in loads[0]:
        copy.start()

    def turned(value):
        return pltpu.roll(value, odd, 1)

    left = lax.broadcasted_iota(jnp.int32, (odd, TILE), 1) < odd
    whole = [full * n + (n + 1) // 2 for n in range(4)]
    split = [full + (full + hi) * (n // 2) for n in range(4)]
    for j, ref in enumerate((gs_ref, us_ref)):
        row = jnp.broadcast_to(ref[pl.ds(full + (full + hi) * lax.div(q, 2), 1), :], (8, TILE))
        row = jnp.where(lax.rem(q, 2) == 0, row, turned(row))
        scl[j : j + 1, :TILE] = row[0:1]
        for i in range(full):
            at_tile = full * q + lax.div(q + 1, 2) + i
            scl[j : j + 1, (i + 1) * TILE : (i + 2) * TILE] = ref[pl.ds(at_tile, 1), :]

    for copy in loads[1]:
        copy.start()
    load_d.start()
    load_x.start()

    def rounded(cls):
        def tile(i):
            if cls == 2:
                return accu[i * TILE : (i + 1) * TILE, :TILE]
            top = (cls * len(cuts) + i // hi) * TILE
            return accg[top : top + TILE, i % hi * TILE : (i % hi + 1) * TILE]

        for n in range(4):
            both = tile(split[n])
            top, low = both[:odd], both[odd:]
            if cls == 2:
                half_tile = top if n % 2 == 0 else low
            elif n % 2 == 0:
                half_tile = jnp.where(left, top, turned(low))
            else:
                half_tile = jnp.where(left, turned(top), low)
            sends[cls][n, :odd] = half_tile.astype(jnp.bfloat16)
            for i in range(full):
                here = slice(odd + i * TILE, odd + (i + 1) * TILE)
                sends[cls][n, here] = tile(whole[n] + i).astype(jnp.bfloat16)
        if cls == 2:
            wd[f] = sends[cls][q]
        else:
            slot[cls][f, TILE:] = sends[cls][q]

    def unfold(i):
        for where in (wg, wu):
            folded = where[i, TILE : TILE + odd].astype(jnp.float32)
            where[i, :odd] = jnp.where(left, folded, 0.0).astype(jnp.bfloat16)
            where[i, odd:TILE] = jnp.where(left, turned(folded), 0.0).astype(jnp.bfloat16)

    def cut(cls, i):
        return wd.at[i] if cls == 2 else slot[cls].at[i, pl.ds(TILE, part)]

    def rsh(cls, k):
        return rcopy(
            sends[cls].at[qk[k]], cut(cls, f),
            rsh_send.at[cls, k - 1], rsh_recv.at[cls, k - 1], at(k),
        )

    def rsh_start(cls, k):
        rsh(cls, k).start()

    def rsh_wait(cls, k):
        where = cut(cls, 4 * z + qk[k])
        rcopy(where, where, rsh_send.at[cls, k - 1], rsh_recv.at[cls, k - 1], at(k)).wait_recv()

    def zcopy(cls, i, d):
        dev = (f + 4, c) if d == 0 else (f - 4, c)
        return rcopy(cut(cls, i), cut(cls, i), z_send.at[d, cls, i], z_recv.at[cls, i], dev)

    def inward(cls, i):
        pl.when(z < 2)(lambda: zcopy(cls, i, 0).start())
        pl.when(z > 1)(lambda: zcopy(cls, i, 1).start())

    def outward(cls, i):
        pl.when(z == 2)(lambda: zcopy(cls, i, 0).start())
        pl.when(z == 1)(lambda: zcopy(cls, i, 1).start())

    inner, outer = (z == 1) | (z == 2), (z == 0) | (z == 3)

    def relay(cls, r, ks, who=None):
        who = z >= 0 if who is None else who
        for k in ks:
            j = qk[k] if cls < 2 else k
            low, high = 4 * (z - r) + j, 4 * (z + r) + j

            @pl.when(who & (z >= r))
            def _():
                zcopy(cls, low, 0).wait_recv()
                if r < 3:
                    pl.when(z < 3)(lambda: zcopy(cls, low, 0).start())

            @pl.when(who & (z + r <= 3))
            def _():
                zcopy(cls, high, 1).wait_recv()
                if r < 3:
                    pl.when(z > 0)(lambda: zcopy(cls, high, 1).start())

    for copy in loads[0]:
        copy.wait()
    rounded(0)
    pl.semaphore_wait(barrier, 4 + jnp.minimum(z, 1) + jnp.minimum(3 - z, 1))
    outward(0, f)
    inward(0, f)
    for k in (1, 2, 3):
        rsh_start(0, k)
    for copy in loads[1]:
        copy.wait()
    rounded(1)
    outward(1, f)
    inward(1, f)
    for k in (1, 2, 3):
        rsh_start(1, k)
    load_d.wait()
    rounded(2)
    for k in (1, 2, 3):
        rsh_start(2, k)
    def both(r, ks):
        for k in ks:
            relay(0, r, (k,))
            relay(1, r, (k,))

    def piece(core, h):
        return pl.ds(pl.multiple_of(half * core + h * quarter, 16), quarter)

    def xcopy(owner, h, ssem, rsem, dev):
        where = xbuf.at[qk[owner], piece(c, h), :]
        return rcopy(where, where, ssem, rsem, dev)

    def direct(k, h, owner):
        return xcopy(owner, h, x_send.at[k - 1, h], x_recv.at[k - 1, h], at(k))

    def onward(h, owner):
        return xcopy(owner, h, x_send.at[2, h], x_recv.at[2, h], at(2 if h == 0 else 1))

    def share(k, h, core):
        where = xbuf.at[qk[k], piece(core, h), :]
        return rcopy(where, where, s_send.at[k, h], s_recv.at[k, h], partner)

    def own_plane(cls):
        for k in (1, 2, 3):
            rsh_wait(cls, k)
            outward(cls, 4 * z + qk[k])
            inward(cls, 4 * z + qk[k])

    own_plane(0)
    load_x.wait()

    def normalize(m, _):
        here = pl.ds(pl.multiple_of(half * c + m * 16, 16), 16)
        values = xbuf[q, here, :].astype(jnp.float32)
        scale = lax.rsqrt(jnp.mean(values * values, axis=-1, keepdims=True) + 1e-06)
        xbuf[q, here, :] = (values * scale * ng_ref[...]).astype(jnp.bfloat16)
        return 0

    lax.fori_loop(0, half // 16, normalize, 0)

    direct(1, 0, 0).start()
    direct(2, 1, 0).start()
    direct(1, 1, 0).start()
    direct(2, 0, 0).start()
    for h in (0, 1):
        share(0, h, c).start()
    own_plane(1)

    side = lax.div(z, 2)
    zz = z + side * (3 - 2 * z)

    def turn(t):
        base = t if t >= 2 else lax.rem(t + zz, 2)
        return base + side * (3 - 2 * base)

    def columns(s, h=None):
        if h is None:
            return pl.ds(pl.multiple_of(s * width, TILE), width)
        return pl.ds(pl.multiple_of(s * width + h * pair, TILE), pair)

    def gate_up(t, k0, k1, portion=None, fresh=True):
        s = turn(t)
        if portion is None:
            blocks, across = [4 * s + i for i in range(4)], columns(s)
        else:
            side = lax.rem(lax.div(q, 2) + portion, 2)
            blocks, across = [4 * s + 2 * side + i for i in (0, 1)], columns(s, side)

        if fresh:
            for i in blocks:
                unfold(i)

        def step(m, _):
            who = chip(lax.div(m, hi // 2))
            n = lax.rem(m, hi // 2)
            here = pl.ds(pl.multiple_of(who * rows, 16), rows)
            cols = pl.ds(pl.multiple_of(n * pair, TILE), pair)
            one = pl.ds(pl.multiple_of(n * pair + odd * jnp.minimum(n, 1), odd), TILE)
            two = pl.ds(pl.multiple_of(n * pair + TILE + odd, odd), TILE)
            found = []
            for j, acc in enumerate((accg, accu)):
                w = jnp.concatenate([
                    jnp.concatenate([slot[j][i, one, :], slot[j][i, two, :]], axis=1) for i in blocks
                ], axis=0)
                x = xbuf[who, :, across]
                part_sum = lax.dot_general(x, w, NN, preferred_element_type=jnp.float32)
                if t > 0:
                    part_sum = part_sum + acc[here, cols]
                if portion != 1:
                    acc[here, cols] = part_sum
                found.append(part_sum)
            if portion == 1:
                g = found[0] * scl[0:1, cols]
                u = found[1] * scl[1:2, cols]
                hid[here, cols] = (g / (1.0 + jnp.exp(-g)) * u).astype(jnp.bfloat16)
            return 0

        lax.fori_loop(k0 * (hi // 2), k1 * (hi // 2), step, 0)

    both(1, range(4))
    for h in (0, 1):
        share(0, h, 1 - c).wait_recv()
    direct(1, 0, 1).wait_recv()
    onward(0, 1).start()
    share(1, 0, c).start()
    direct(2, 1, 2).wait_recv()
    onward(1, 2).start()
    share(2, 1, c).start()
    for k in (1, 2, 3):
        rsh_wait(2, k)
    for j in range(4):
        inward(2, 4 * z + j)
    both(2, range(3))
    direct(1, 1, 1).wait_recv()
    share(1, 1, c).start()
    direct(2, 0, 2).wait_recv()
    share(2, 0, c).start()
    for k in (1, 2):
        for h in (0, 1):
            share(k, h, 1 - c).wait_recv()
    gate_up(0, 0, 3)
    both(2, (3,))
    for j in range(4):
        outward(2, 4 * z + j)
    gate_up(1, 0, 3)
    gate_up(2, 0, 3)
    onward(0, 3).wait_recv()
    share(3, 0, c).start()
    onward(1, 3).wait_recv()
    share(3, 1, c).start()
    for h in (0, 1):
        share(3, h, 1 - c).wait_recv()
    for t in range(3):
        gate_up(t, 3, 4, None, False)
    for h in (0, 1):
        direct(1, h, 0).wait_send()
        direct(2, h, 0).wait_send()
        onward(h, 1 + h).wait_send()
        for k in range(4):
            share(k, h, c).wait_send()
    def spot(u):
        s = turn(u // 2)
        return 2 * lax.rem(s, 2) + u % 2, columns(s, u % 2), lax.div(s, 2)

    def pcopy(i, cols, k):
        return rcopy(
            xbuf.at[chip(k), :, cols], pbuf.at[i, k], p_send.at[i, k], p_recv.at[i, k], partner
        )

    def product(u, k):
        i, cols, owner = spot(u)
        block = 4 * turn(u // 2) + 2 * (u % 2)
        here = pl.ds(pl.multiple_of(chip(k) * rows, 16), rows)
        nothing = jnp.zeros((TILE - odd, TILE), jnp.bfloat16)
        w = jnp.concatenate([
            jnp.concatenate([wd[block + n, :odd], nothing, wd[block + n, odd:]], axis=0) for n in (0, 1)
        ], axis=1)
        o = lax.dot_general(hid[here, :], w, NN, preferred_element_type=jnp.float32)
        xbuf[chip(k), :, cols] = o.astype(jnp.bfloat16)
        pl.when(owner != c)(lambda: pcopy(i, cols, k).start())

    def products(u):
        def step(n, _):
            product(u, 3 - n)
            return 0

        lax.fori_loop(0, 4, step, 0)

    places = ((1, 0, 1), (3, 0, 1), (2, 1, 2), (3, 1, 2), (2, 0, 2), (1, 1, 1))

    def scopy(i, cols, place):
        k, h, to = places[place]
        return rcopy(
            xbuf.at[qk[k], pl.ds(h * half, half), cols], rbuf.at[i, place],
            r_send.at[i, place], r_recv.at[i, place], at(to),
        )

    def added(k, first_row, n_rows, cols, more):
        who = chip(k)

        def step(m, _):
            here = pl.ds(pl.multiple_of(first_row + m * TILE, 16), TILE)
            there = pl.ds(pl.multiple_of(m * TILE, 16), TILE)
            both = xbuf[who, here, cols].astype(jnp.float32) + more[there, :].astype(jnp.float32)
            xbuf[who, here, cols] = both.astype(jnp.bfloat16)
            return 0

        lax.fori_loop(0, n_rows // TILE, step, 0)

    def finish(u, k):
        i, cols, owner = spot(u)

        @pl.when(owner == c)
        def _():
            pcopy(i, cols, k).wait_recv()
            added(k, 0, rows, cols, pbuf.at[i, k])

            @pl.when(k == 3)
            def _():
                scopy(i, cols, 1).start()
                scopy(i, cols, 3).start()

            pl.when(k == 2)(lambda: scopy(i, cols, 2).start())
            pl.when(k == 1)(lambda: scopy(i, cols, 0).start())

    def finish_all(u):
        def step(n, _):
            finish(u, 3 - n)
            return 0

        lax.fori_loop(0, 4, step, 0)

    def second(u):
        i, cols, owner = spot(u)

        @pl.when(owner == c)
        def _():
            for came, goes in ((1, 4), (3, 5)):
                scopy(i, cols, came).wait_recv()
                k, h, _ = places[goes]
                added(k, h * half, half, cols, rbuf.at[i, came])
                scopy(i, cols, goes).start()

    def final(u):
        i, cols, owner = spot(u)

        @pl.when(owner == c)
        def _():
            there = pl.ds(pl.multiple_of(i * pair, TILE), pair)
            for h, (one, two) in enumerate(((0, 4), (2, 5))):
                scopy(i, cols, one).wait_recv()
                scopy(i, cols, two).wait_recv()

                def step(m, _):
                    here = pl.ds(pl.multiple_of(h * half + m * TILE, 16), TILE)
                    part = pl.ds(pl.multiple_of(m * TILE, 16), TILE)
                    total = (
                        xbuf[q, here, cols].astype(jnp.float32)
                        + rbuf[i, one, part, :].astype(jnp.float32)
                        + rbuf[i, two, part, :].astype(jnp.float32)
                    )
                    out_ref[here, there] = (total * ds_ref[:, there]).astype(jnp.bfloat16)
                    return 0

                lax.fori_loop(0, half // TILE, step, 0)

    both(3, (0, 1))
    gate_up(3, 0, 4, 0)
    both(3, (2, 3))
    for i in (0, 1):
        unfold(4 * turn(3) + 2 * lax.rem(lax.div(q, 2) + 1, 2) + i)

    def begin(n, _):
        gate_up(3, 3 - n, 4 - n, 1, False)
        product(0, 3 - n)
        pl.when(n > 0)(lambda: finish(0, 4 - n))
        return 0

    lax.fori_loop(0, 4, begin, 0)
    finish(0, 0)
    products(1)
    finish_all(1)
    second(0)
    for u in range(2, 7):
        relay(2, u // 2, (2 * (u % 2), 2 * (u % 2) + 1))
        products(u)
        finish_all(u)
        second(u - 1)
        if u > 3:
            final(u - 4)
    relay(2, 3, (2, 3))
    products(7)
    finish_all(7)
    second(6)
    for u in range(3, 6):
        final(u)
    second(7)
    final(6)
    final(7)

    for cls in (0, 1, 2):
        for k in (1, 2, 3):
            rsh(cls, k).wait_send()
        for r in range(3):
            for k in range(4):
                low, high = 4 * (z - r) + qk[k], 4 * (z + r) + qk[k]
                pl.when((z >= r) & (z < 3))(
                    lambda: zcopy(cls, low, 0).wait_send()
                )
                pl.when((z + r <= 3) & (z > 0))(
                    lambda: zcopy(cls, high, 1).wait_send()
                )
    for u in range(8):
        i, cols, owner = spot(u)

        @pl.when(owner == c)
        def _():
            for place in range(6):
                scopy(i, cols, place).wait_send()

        @pl.when(owner != c)
        def _():
            for k in range(4):
                pcopy(i, cols, k).wait_send()


def planes(tokens, norm_gain, gate_weight, up_weight, gate_scale, up_scale, down_weight, down_scale):
    rows, model = tokens.shape
    units = gate_weight.shape[1]
    tiles, part = units // TILE, units // 4
    hi = -(-part // TILE)
    bf, f32, dma = jnp.bfloat16, jnp.float32, pltpu.SemaphoreType.DMA
    hbm = pl.BlockSpec(memory_space=pl.ANY)
    vmem = pl.BlockSpec(memory_space=pltpu.VMEM)
    return pl.pallas_call(
        kernel,
        out_shape=jax.ShapeDtypeStruct((rows, down_scale.shape[0]), bf),
        in_specs=[hbm, hbm, hbm, hbm, vmem, vmem, vmem, vmem],
        out_specs=vmem,
        scratch_shapes=[
            pltpu.VMEM((4, rows, model), bf),
            pltpu.VMEM((16, TILE + part, TILE), bf),
            pltpu.VMEM((16, TILE + part, TILE), bf),
            pltpu.VMEM((16, part, TILE), bf),
            pltpu.VMEM((4, part, TILE), bf),
            pltpu.VMEM((4, part, TILE), bf),
            pltpu.VMEM((4, part, TILE), bf),
            pltpu.VMEM((4 * rows, hi * TILE), f32),
            pltpu.VMEM((4 * rows, hi * TILE), f32),
            pltpu.VMEM((4 * rows, hi * TILE), bf),
            pltpu.VMEM((4, 4, rows, 2 * TILE), bf),
            pltpu.VMEM((4, 6, rows // 2, 2 * TILE), bf),
            pltpu.VMEM((8, hi * TILE), f32),
            dma((3, 4)), dma((3, 3)), dma((3, 3)),
            dma((3, 2)), dma((3, 2)), dma((4, 2)), dma((4, 2)),
            dma((2, 3, 16)), dma((3, 16)),
            dma((4, 4)), dma((4, 4)), dma((4, 6)), dma((4, 6)),
        ],
        compiler_params=pltpu.CompilerParams(
            collective_id=0, has_side_effects=True, vmem_limit_bytes=67043328
        ),
    )(
        gate_weight, up_weight, down_weight, tokens,
        norm_gain[None], gate_scale.reshape(tiles, TILE), up_scale.reshape(tiles, TILE), down_scale[None],
    )


def solution(mesh):
    in_specs = (
        P("fs", None),
        P(),
        P("fs", "tp"),
        P("fs", "tp"),
        P("tp"),
        P("tp"),
        P("tp", "fs"),
        P("tp"),
    )
    out_specs = P("fs", "tp")
    body = planes if (mesh.shape["fs"], mesh.shape["tp"]) == (16, 2) else gathered
    return jax.shard_map(body, mesh=mesh, in_specs=in_specs, out_specs=out_specs, check_vma=False)
```

time: 181 us -> 166 us (0.917)
  Pallas kernels: 175 us -> 163 us
  local copies, waits for them, and re-layouts: 5.29 us -> 2.67 us
    pallas_call x1, Pallas kernels: 175 us -> 163 us  [planes(): pl.pallas_call(kernel, out_shape=jax.ShapeDtypeStruct((rows, down_scale.s...]
    broadcast_in_dim x2 -> x0, local copies, waits for them, and re-layouts: 2.62 us -> none  [the longest x1 1.31 us: planes(): gate_scale[None]]
where the time goes in v2:
time: 166 us
  Pallas kernels  163 us (98%)
  local copies, waits for them, and re-layouts  2.67 us (2%)
    pallas_call x1, Pallas kernels, planes(): pl.pallas_call(kernel, out_shape=jax.ShapeDtypeStruct((rows, down_scale.s...  163 us

profile of v2, /device:TPU:1, one launch (start us, length us, event | category | flops | bytes accessed | tf_op | source)
XLA Modules:
  0.0 165.8 jit_solution(15749443834108280979)
XLA Ops:
  0.0 163.1 %shard_map.82 = bf16[768,1024]{1,0:T(8,128)(2,1)} custom-call(f32[128,2816]{1,0:T(8,128)} %g_ref.1, f32[128,2816]{1,0:T(8,128)} %u_ref.1, f32[2816,128]{1,0:T(8,128)} %d_ref.1, bf16[768,2048]{1,0:T(8,128)(2,1)} %x_ref.1, f32[1,2048]{1,0:T(1,128)} %bitcast.6, f32[22,128]{1,0:T(8,128)} %bitcast.4, f32[22,128]{1,0:T(8,128)} %bitcast.5, f32[1,1024]{1,0:T(1,128)} %bitcast.7), custom_call_target="tpu_custom_call" | custom-call | tf_op jit(solution)/shard_map/pallas_call | solution.py:531
  163.1 2.7 %copy.10 = bf16[768,1024]{1,0:T(8,128)(2,1)} copy(bf16[768,1024]{1,0:T(8,128)(2,1)} %shard_map.82) | data formatting | bytes 3145728

commit v3 on v2

--- a/solution.py
+++ b/solution.py
@@ -437,6 +437,10 @@
                 added(k, h * half, half, cols, rbuf.at[i, came])
                 scopy(i, cols, goes).start()
 
+    def result(i, cols):
+        there = pl.ds(pl.multiple_of(i * pair, TILE), pair)
+        return pltpu.make_async_copy(xbuf.at[q, :, cols], out_ref.at[:, there], l_sem.at[0, i])
+
     def final(u):
         i, cols, owner = spot(u)
 
@@ -455,10 +459,11 @@
                         + rbuf[i, one, part, :].astype(jnp.float32)
                         + rbuf[i, two, part, :].astype(jnp.float32)
                     )
-                    out_ref[here, there] = (total * ds_ref[:, there]).astype(jnp.bfloat16)
+                    xbuf[q, here, cols] = (total * ds_ref[:, there]).astype(jnp.bfloat16)
                     return 0
 
                 lax.fori_loop(0, half // TILE, step, 0)
+            result(i, cols).start()
 
     both(3, (0, 1))
     gate_up(3, 0, 4, 0)
@@ -511,6 +516,7 @@
 
         @pl.when(owner == c)
         def _():
+            result(i, cols).wait()
             for place in range(6):
                 scopy(i, cols, place).wait_send()
 
@@ -518,6 +524,25 @@
         def _():
             for k in range(4):
                 pcopy(i, cols, k).wait_send()
+
+
+def handed_on(in_ref, out_ref, held, in_sem, out_sem):
+    pieces = in_sem.shape[0]
+    rows = held.shape[0] // pieces
+
+    def copies(n, out):
+        here = pl.ds(n * rows, rows)
+        if out:
+            return pltpu.make_async_copy(held.at[here, :], out_ref.at[here, :], out_sem.at[n])
+        return pltpu.make_async_copy(in_ref.at[here, :], held.at[here, :], in_sem.at[n])
+
+    for n in range(pieces):
+        copies(n, False).start()
+    for n in range(pieces):
+        copies(n, False).wait()
+        copies(n, True).start()
+    for n in range(pieces):
+        copies(n, True).wait()
 
 
 def planes(tokens, norm_gain, gate_weight, up_weight, gate_scale, up_scale, down_weight, down_scale):
@@ -528,11 +553,11 @@
     bf, f32, dma = jnp.bfloat16, jnp.float32, pltpu.SemaphoreType.DMA
     hbm = pl.BlockSpec(memory_space=pl.ANY)
     vmem = pl.BlockSpec(memory_space=pltpu.VMEM)
-    return pl.pallas_call(
+    summed = pl.pallas_call(
         kernel,
         out_shape=jax.ShapeDtypeStruct((rows, down_scale.shape[0]), bf),
         in_specs=[hbm, hbm, hbm, hbm, vmem, vmem, vmem, vmem],
-        out_specs=vmem,
+        out_specs=hbm,
         scratch_shapes=[
             pltpu.VMEM((4, rows, model), bf),
             pltpu.VMEM((16, TILE + part, TILE), bf),
@@ -559,6 +584,14 @@
         gate_weight, up_weight, down_weight, tokens,
         norm_gain[None], gate_scale.reshape(tiles, TILE), up_scale.reshape(tiles, TILE), down_scale[None],
     )
+    pieces = 4
+    return pl.pallas_call(
+        handed_on,
+        out_shape=jax.ShapeDtypeStruct(summed.shape, bf),
+        in_specs=[hbm],
+        out_specs=hbm,
+        scratch_shapes=[pltpu.VMEM(summed.shape, bf), dma((pieces,)), dma((pieces,))],
+    )(summed)
 
 
 def solution(mesh):

time: 166 us -> 165 us (level)
  local copies, waits for them, and re-layouts: 2.67 us -> 0 us
  Pallas kernels: 163 us -> 165 us
    unnamed x1 -> x0, local copies, waits for them, and re-layouts: 2.67 us -> none
    pallas_call x0 -> x1, Pallas kernels: none -> 2.2 us  [planes(): pl.pallas_call(handed_on, out_shape=jax.ShapeDtypeStruct(summed.shape, bf...]
where the time goes in v3:
time: 165 us
  Pallas kernels  165 us (100%)
    pallas_call x1, Pallas kernels, planes(): pl.pallas_call(kernel, out_shape=jax.ShapeDtypeStruct((rows, down_scale.s...  162 us

profile of v3, /device:TPU:1, one launch (start us, length us, event | category | flops | bytes accessed | tf_op | source)
XLA Modules:
  0.0 164.7 jit_solution(8576928382913500118)
XLA Ops:
  0.0 162.5 %shard_map.82.in_ref = bf16[768,1024]{1,0:T(8,128)(2,1)} custom-call(f32[128,2816]{1,0:T(8,128)} %g_ref.1, f32[128,2816]{1,0:T(8,128)} %u_ref.1, f32[2816,128]{1,0:T(8,128)} %d_ref.1, bf16[768,2048]{1,0:T(8,128)(2,1)} %x_ref.1, f32[1,2048]{1,0:T(1,128)} %bitcast.6, f32[22,128]{1,0:T(8,128)} %bitcast.4, f32[22,128]{1,0:T(8,128)} %bitcast.5, f32[1,1024]{1,0:T(1,128)} %bitcast.7), custom_call_target="tpu_custom_call" | custom-call | tf_op jit(solution)/shard_map/pallas_call | solution.py:556
  162.5 2.2 %shard_map.83 = bf16[768,1024]{1,0:T(8,128)(2,1)} custom-call(bf16[768,1024]{1,0:T(8,128)(2,1)} %shard_map.82.in_ref), custom_call_target="tpu_custom_call" | custom-call | tf_op jit(solution)/shard_map/pallas_call | solution.py:588
